TPU v7x, 32 devices: a whole 2x2x4 slice. The times are simulated.
32 devices in a mesh: fs: 8 (over z, y), tp: 4 (over x, core).
Axes of the slice: x: 2, y: 2, z: 4, core: 2. Of those that a mesh axis runs over, the one named last changes fastest.
Arguments:
- tokens: bfloat16 [6144, 2048], P('fs'), may hold values from -6 to 6
- norm_gain: float32 [2048], P('fs'), may hold values from 0.1 to 1.9
- gate_weight: float32 [2048, 5632], P('fs', 'tp'), may hold values from -0.125 to 0.125
- up_weight: float32 [2048, 5632], P('fs', 'tp'), may hold values from -0.125 to 0.125
- down_weight: float32 [5632, 2048], P('fs', 'tp'), may hold values from -0.078125 to 0.078125
Outputs:
- gate_out: bfloat16 [2048, 5632], P(None, 'tp')
- up_out: bfloat16 [2048, 5632], P(None, 'tp')
- down_out: bfloat16 [5632, 2048], P('tp')
- mixed: bfloat16 [6144, 2048], P('fs', 'tp')
All inputs are finite; a program needn't handle non-finite values.
Results may differ from a plain program's by a relative error of at most 0.0095.
Values may be sent and summed in bfloat16 or wider, within the bound.
A program may use at most 128 MiB of HBM per device.

v0:
```python
import functools

import jax
import jax.numpy as jnp
from jax import lax
from jax.experimental import pallas as pl
from jax.experimental.pallas import tpu as pltpu
from jax.sharding import PartitionSpec as P

eps_norm = 1e-06
MESH = pl.DeviceIdType.MESH

PIECES = (
    ("gate", 0, 1, "a"),
    ("gate", 1, 1, "a"),
    ("down", 2, 2, "b"),
    ("up", 0, 1, "a"),
    ("up", 1, 1, "a"),
    ("down", 0, 1, "a"),
    ("down", 1, 1, "a"),
)
PHASES = ((0, 1, 6), (2,), (3, 4), (5,))
GROUPS = ((1, 3, (2, 6)), (0, 1, (5,)))


def cost(p):
    return 0.5 if PIECES[p][0] == "down" and kind(p) == 1 else 1.0


def kind(p):
    return PIECES[p][3]


def plan(n_z):
    events = []
    seq = [(d, p) for phase in PHASES for d in range(1, n_z) for p in phase]
    order = sorted(range(len(PIECES)), key=lambda p: kind(p) == "a")
    own, total = {}, 0.0
    for p in order:
        total += cost(p)
        own[p] = total
    z_time, now = {}, 0.0
    for i, phase in enumerate(PHASES):
        for d in range(1, n_z):
            if d == n_z - 1 and i + 1 < len(PHASES):
                events.append((now + 0.02, 1, "launch", i + 1, 0))
            for p in phase:
                if kind(p) == "a":
                    now += cost(p)
                    z_time[d, p] = now
                    events.append((now, 0, "line", d, p))
                else:
                    now += 2.0 * cost(p)
                    z_time[d, p] = now
                    events.append((now - cost(p), 0, "line", d, p))
                    events.append((now, 0, "line_other", d, p))
    y_time = {}
    for z in range(n_z):
        at = total
        for d, p in seq:
            if kind(p) == "a":
                for zz in (z - d, z + d):
                    if 0 <= zz < n_z:
                        at = max(at, z_time[d, p]) + cost(p)
                        y_time[d, p] = max(y_time.get((d, p), 0.0), at)
    for p, at in own.items():
        events.append((at, 1, "pair", 0, p))
    for (d, p), at in y_time.items():
        events.append((at, 1, "pair", d, p))
    here = dict(y_time)
    here.update({(0, p): at for p, at in own.items()})
    last = 0.0
    for name in ("gate", "up"):
        mine = [p for p in range(len(PIECES)) if PIECES[p][0] == name]
        for d in range(n_z):
            at = max(here[d, p] for p in mine) + 0.01
            events.append((at, 2, "mul_" + name, d, 0))
            last = max(last, at)
    events.append((last + 0.01, 3, "act", 0, 0))
    end = max(e[0] for e in events) + 0.1
    for step in range(4):
        events.append((end + 0.01 + 0.01 * step, 4, "share", 0, step))
    for step in range(5):
        events.append((end + 0.1 + 0.1 * step, 4, "share", 1, step))
    events.append((end + 0.35, 4, "share", 0, 4))
    return sorted(events)


def kernel(
    n_fs, n_tp, tok_hbm, gain, gw, uw, dw, gate_o, up_o, down_o, mix_o,
    tok, dcol, normed, acc_g, acc_u, hidden, share0, share1, pair0, pair1, send0, send1, in0, in1,
    tok_sem, ag_send, ag_recv, aa_send, aa_recv, rs_send, rs_recv,
):
    tok_copy = pltpu.make_async_copy(tok_hbm, tok, tok_sem)
    tok_copy.start()
    shares, pairs, sends, ins = (share0, share1), (pair0, pair1), (send0, send1), (in0, in1)
    f, t = lax.axis_index("fs"), lax.axis_index("tp")
    n_z = n_fs // 2
    z, y = f // 2, f % 2
    per = n_fs // n_tp
    rows = gw.shape[0]
    d_rows, d_cols = dw.shape
    part = d_cols // 4
    n_tok = tok.shape[0]
    k_z = normed.shape[2]
    m_tile = min(256, n_tok)
    width = gw.shape[1]
    col_tiles = [(c, min(512, width - c)) for c in range(0, width, 512)]

    def flip(bit):
        return t + bit - 2 * bit * ((t // bit) % 2)

    near, far = flip(1), flip(2)
    far_near = far + 1 - 2 * (far % 2)

    def view(o, p):
        name, h, n, _ = PIECES[p]
        if name == "down":
            return dcol.at[o, :, pl.ds(h * part, n * part)]
        ref = gate_o if name == "gate" else up_o
        return ref.at[pl.ds(pl.multiple_of(o * rows + h * (rows // 2), rows // 2), rows // 2), :]

    def ag(o, p, way, dest):
        v = view(o, p)
        return pltpu.make_async_remote_copy(
            v, v, ag_send.at[o, p, way], ag_recv.at[o, p],
            device_id=(dest, t), device_id_type=MESH,
        )

    started = []

    def start(cond, make):
        if cond is None:
            make().start()
        else:
            pl.when(cond)(lambda: make().start())
        started.append((cond, make))

    def land(o, p):
        ag(o, p, 0, f).wait_recv()

    def exchange(cond, o, p):
        name, h, n, _ = PIECES[p]
        if name != "down":
            return
        owner = o // per
        k = o % per
        row = pl.multiple_of(k * d_rows, d_rows)
        col = pl.multiple_of(t * d_cols + h * part, part)

        def make():
            return pltpu.make_async_remote_copy(
                view(o, p), down_o.at[pl.ds(row, d_rows), pl.ds(col, n * part)],
                aa_send.at[o, p], aa_recv.at[t, k, p],
                device_id=(f, owner), device_id_type=MESH,
            )

        away = owner != t
        start(away if cond is None else jnp.logical_and(cond, away), make)
        mine = owner == t

        @pl.when(mine if cond is None else jnp.logical_and(cond, mine))
        def _():
            down_o[pl.ds(row, d_rows), pl.ds(col, n * part)] = dcol[o, :, h * part : (h + n) * part]

    barrier = pltpu.get_barrier_semaphore()
    other_y = f + 1 - 2 * y
    peers = [
        (z > 0, (f - 2, t)), (z < n_z - 1, (f + 2, t)), (None, (other_y, t)),
        (None, (f, near)), (None, (f, far)), (None, (f, far_near)),
    ]
    for cond, dev in peers:
        def hello(dev=dev):
            pl.semaphore_signal(barrier, inc=1, device_id=dev, device_id_type=MESH)
        hello() if cond is None else pl.when(cond)(hello)

    g = jnp.broadcast_to(gain[...], (8, rows)).T[:, :1]
    base = pl.multiple_of(f * rows, rows)
    gate_o[pl.ds(base, rows), :] = (gw[...] * g).astype(jnp.bfloat16)
    dcol[f] = dw[...].astype(jnp.bfloat16)
    up_o[pl.ds(base, rows), :] = (uw[...] * g).astype(jnp.bfloat16)
    inner = jnp.logical_and(z > 0, z < n_z - 1)
    pl.when(inner)(lambda: pl.semaphore_wait(barrier, len(peers)))
    pl.when(jnp.logical_not(inner))(lambda: pl.semaphore_wait(barrier, len(peers) - 1))

    def launch(phase):
        for p in PHASES[phase]:
            start(z > 0, functools.partial(ag, f, p, 0, f - 2))
            start(z < n_z - 1, functools.partial(ag, f, p, 1, f + 2))
            if kind(p) == "b":
                other_b(p)

    def other_b(p):
        start(z > 0, functools.partial(ag, other_y, p, 0, f - 2))
        start(z < n_z - 1, functools.partial(ag, other_y, p, 1, f + 2))

    for p in sorted(range(len(PIECES)), key=lambda p: kind(p) == "a"):
        start(None, functools.partial(ag, f, p, 2, other_y))
    for p in PHASES[0]:
        start(z > 0, functools.partial(ag, f, p, 0, f - 2))
        start(z < n_z - 1, functools.partial(ag, f, p, 1, f + 2))
    for p in range(len(PIECES)):
        exchange(None, f, p)

    n_norm = n_tok // 64
    tok_copy.wait()

    @pl.loop(0, n_norm)
    def _(i):
        r = pl.multiple_of(i * 64, 64)
        x = tok[pl.ds(r, 64), :].astype(jnp.float32)
        x = x * lax.rsqrt(jnp.mean(x * x, axis=-1, keepdims=True) + eps_norm)
        x = x.astype(jnp.bfloat16)
        for j in range(n_z):
            normed[j, pl.ds(r, 64), :] = x[:, j * k_z : (j + 1) * k_z]

    def multiply(w, acc, zz, first):
        k0 = pl.multiple_of(zz * k_z, k_z)

        @pl.loop(0, n_tok // m_tile)
        def _(i):
            r = pl.multiple_of(i * m_tile, m_tile)
            a = normed[zz, pl.ds(r, m_tile), :]
            for c, n in col_tiles:
                v = jnp.dot(a, w[pl.ds(k0, k_z), c : c + n], preferred_element_type=jnp.float32)
                if first:
                    acc[pl.ds(r, m_tile), c : c + n] = v
                else:
                    acc[pl.ds(r, m_tile), c : c + n] += v

    def sides(d):
        return [(z >= d, z - d, -1), (z + d < n_z, z + d, 1)]

    def forward(cond, zz, sign, o, p):
        if sign < 0:
            start(jnp.logical_and(cond, z < n_z - 1), functools.partial(ag, o, p, 1, f + 2))
        else:
            start(jnp.logical_and(cond, z > 0), functools.partial(ag, o, p, 0, f - 2))

    def share_step(group, step):
        q, n, parts = GROUPS[group]
        share, half_in, out_send, out_in = shares[group], pairs[group], sends[group], ins[group]
        wide = n * part

        def aa_wait(c):
            for k in range(per):
                for p in parts:
                    _, h, m, _ = PIECES[p]
                    ref = down_o.at[
                        pl.ds(k * d_rows, d_rows), pl.ds(pl.multiple_of(c * d_cols + h * part, part), m * part)
                    ]
                    pltpu.make_async_remote_copy(
                        ref, ref, aa_send.at[0, p], aa_recv.at[c, k, p], device_id=(f, near), device_id_type=MESH,
                    ).wait_recv()

        def product(c, slot):
            @pl.loop(0, n_tok // m_tile)
            def _(i):
                r = pl.multiple_of(i * m_tile, m_tile)
                col = pl.multiple_of(c * d_cols + q * part, part)
                v = jnp.dot(hidden[pl.ds(r, m_tile), :], down_o[:, pl.ds(col, wide)], preferred_element_type=jnp.float32)
                share[slot, pl.ds(r, m_tile), :] = v.astype(jnp.bfloat16)

        def pair(slot):
            return pltpu.make_async_remote_copy(
                share.at[slot], half_in.at[slot], rs_send.at[group, slot], rs_recv.at[group, slot],
                device_id=(f, near), device_id_type=MESH,
            )

        def across():
            return pltpu.make_async_remote_copy(
                out_send, out_in, rs_send.at[group, 2], rs_recv.at[group, 2],
                device_id=(f, far), device_id_type=MESH,
            )

        if step == 0:
            aa_wait(far_near)
            product(far_near, 0)
            start(None, functools.partial(pair, 0))
        elif step == 1:
            aa_wait(far)
            product(far, 2)
            pair(0).wait_recv()
            out_send[...] = (share[2].astype(jnp.float32) + half_in[0].astype(jnp.float32)).astype(jnp.bfloat16)
            start(None, across)
        elif step == 2:
            aa_wait(near)
            product(near, 1)
            start(None, functools.partial(pair, 1))
        elif step == 3:
            product(t, 3)
        elif step == 4:
            pair(1).wait_recv()
            across().wait_recv()
            mix_o[:, q * part : (q + n) * part] = (
                share[3].astype(jnp.float32) + half_in[1].astype(jnp.float32) + out_in[...].astype(jnp.float32)
            ).astype(jnp.bfloat16)

    for _, _, what, d, p in plan(n_z):
        if what == "launch":
            launch(d)
        elif what == "share":
            share_step(d, p)
        elif what == "line":
            for cond, zz, sign in sides(d):
                o = zz * 2 + y
                pl.when(cond)(functools.partial(land, o, p))
                forward(cond, zz, sign, o, p)
                if kind(p) == "a":
                    start(cond, functools.partial(ag, o, p, 2, other_y))
                exchange(cond, o, p)
        elif what == "line_other":
            for cond, zz, sign in sides(d):
                o = zz * 2 + 1 - y
                pl.when(cond)(functools.partial(land, o, p))
                forward(cond, zz, sign, o, p)
                exchange(cond, o, p)
        elif what == "pair":
            if d == 0:
                land(other_y, p)
                exchange(None, other_y, p)
            else:
                for cond, zz, sign in sides(d):
                    o = zz * 2 + 1 - y
                    pl.when(cond)(functools.partial(land, o, p))
                    exchange(cond, o, p)
        elif what == "mul_gate" or what == "mul_up":
            w, acc = (gate_o, acc_g) if what == "mul_gate" else (up_o, acc_u)
            if d == 0:
                multiply(w, acc, z, True)
            else:
                for cond, zz, sign in sides(d):
                    pl.when(cond)(functools.partial(multiply, w, acc, zz, False))
        elif what == "act":
            @pl.loop(0, n_tok // 32)
            def _(i):
                r = pl.multiple_of(i * 32, 32)
                v = acc_g[pl.ds(r, 32), :]
                hidden[pl.ds(r, 32), :] = (v / (1.0 + jnp.exp(-v)) * acc_u[pl.ds(r, 32), :]).astype(jnp.bfloat16)

    for cond, make in started:
        if cond is None:
            make().wait_send()
        else:
            pl.when(cond)(lambda make=make: make().wait_send())


def on_device(n_fs, n_tp, tokens, norm_gain, gate_weight, up_weight, down_weight):
    n_tok, d_model = tokens.shape
    rows, width = gate_weight.shape
    d_rows, d_cols = down_weight.shape
    part = d_cols // 4
    n_z = n_fs // 2
    n_p = len(PIECES)
    bf = jnp.bfloat16
    vmem = pl.BlockSpec(memory_space=pltpu.VMEM)
    dma = pltpu.SemaphoreType.DMA
    return pl.pallas_call(
        functools.partial(kernel, n_fs, n_tp),
        out_shape=(
            pltpu.VMEM((d_model, width), bf),
            pltpu.VMEM((d_model, width), bf),
            pltpu.VMEM((d_rows * n_fs // n_tp, d_model), bf),
            pltpu.VMEM((n_tok, d_cols), bf),
        ),
        in_specs=[pl.BlockSpec(memory_space=pl.ANY)] + [vmem] * 4,
        out_specs=(vmem,) * 4,
        scratch_shapes=[
            pltpu.VMEM((n_tok, d_model), bf),
            pltpu.VMEM((n_fs, d_rows, d_cols), bf),
            pltpu.VMEM((n_z, n_tok, d_model // n_z), bf),
            pltpu.VMEM((n_tok, width), jnp.float32),
            pltpu.VMEM((n_tok, width), jnp.float32),
            pltpu.VMEM((n_tok, width), bf),
            *[pltpu.VMEM((4, n_tok, g[1] * part), bf) for g in GROUPS],
            *[pltpu.VMEM((2, n_tok, g[1] * part), bf) for g in GROUPS],
            *[pltpu.VMEM((n_tok, g[1] * part), bf) for g in GROUPS],
            *[pltpu.VMEM((n_tok, g[1] * part), bf) for g in GROUPS],
            dma,
            dma((n_fs, n_p, 3)),
            dma((n_fs, n_p)),
            dma((n_fs, n_p)),
            dma((n_tp, n_fs // n_tp, n_p)),
            dma((2, 3)),
            dma((2, 3)),
        ],
        compiler_params=pltpu.CompilerParams(
            collective_id=0, has_side_effects=True, vmem_limit_bytes=46 * 2**20
        ),
    )(tokens, norm_gain[None, :], gate_weight, up_weight, down_weight)


def solution(mesh):
    n_fs, n_tp = mesh.shape["fs"], mesh.shape["tp"]
    in_specs = (P("fs", None), P("fs"), P("fs", "tp"), P("fs", "tp"), P("fs", "tp"))
    out_specs = (P(None, "tp"), P(None, "tp"), P("tp", None), P("fs", "tp"))
    return jax.shard_map(
        functools.partial(on_device, n_fs, n_tp), mesh=mesh, in_specs=in_specs, out_specs=out_specs, check_vma=False
    )
```

profile of v0, /device:TPU:0, one launch (start us, length us, event | category | flops | bytes accessed | tf_op | source)
XLA Modules:
  0.0 216.1 jit_solution(1866270889515319469)
XLA Ops:
  0.6 207.0 %shard_map.84 = (bf16[2048,1408]{1,0:T(8,128)(2,1)S(1)}, bf16[2048,1408]{1,0:T(8,128)(2,1)S(1)}, bf16[1408,2048]{1,0:T(8,128)(2,1)S(1)}, bf16[768,512]{1,0:T(8,128)(2,1)S(1)}) custom-call(bf16[768,2048]{1,0:T(8,128)(2,1)} %tok_hbm.1, f32[1,256]{1,0:T(1,128)} %bitcast.1, f32[256,1408]{1,0:T(8,128)} %gw.1, f32[256,1408]{1,0:T(8,128)} %uw.1, f32[704,512]{1,0:T(8,128)} %dw.1), custom_call_target="tpu_custom_call" | custom-call | tf_op jit(solution)/shard_map/pallas_call | solution.py:358
  207.6 2.5 %copy.13 = bf16[2048,1408]{1,0:T(8,128)(2,1)} copy(bf16[2048,1408]{1,0:T(8,128)(2,1)S(1)} %get-tuple-element.4) | data formatting | bytes 11534336
  210.2 0.9 copy.16
  211.1 2.5 %copy.14 = bf16[2048,1408]{1,0:T(8,128)(2,1)} copy(bf16[2048,1408]{1,0:T(8,128)(2,1)S(1)} %get-tuple-element.5) | data formatting | bytes 11534336
  213.6 2.5 %copy.15 = bf16[1408,2048]{1,0:T(8,128)(2,1)} copy(bf16[1408,2048]{1,0:T(8,128)(2,1)S(1)} %get-tuple-element.6) | data formatting | bytes 11534336
where the time goes:
time: 216 us
  Pallas kernels  207 us (96%)
  local copies, waits for them, and re-layouts  8.47 us (4%)
    pallas_call x1, Pallas kernels, on_device(): pl.pallas_call(functools.partial(kernel, n_fs, n_tp), out_shape=(pltpu.VM...  207 us
    unnamed x4, local copies, waits for them, and re-layouts  8.47 us

commit v1 on v0

--- a/solution.py
+++ b/solution.py
@@ -1,4 +1,5 @@
 import functools
+import heapq
 
 import jax
 import jax.numpy as jnp
@@ -390,10 +391,461 @@
     )(tokens, norm_gain[None, :], gate_weight, up_weight, down_weight)
 
 
+PARTS = (
+    ("gate", 0, 8, "a"),
+    ("gate", 8, 8, "a"),
+    ("up", 0, 6, "a"),
+    ("up", 6, 5, "a"),
+    ("up", 11, 5, "b"),
+    ("down", 0, 1, "a"),
+    ("down", 1, 1, "a"),
+    ("down", 2, 1, "a"),
+    ("down", 3, 1, "b"),
+)
+DOWN = tuple(p for p in range(len(PARTS)) if PARTS[p][0] == "down")
+FAR_GROUPS = ((0, 2), (2, 2))
+NEAR_GROUPS = ((0, 2), (2, 1), (3, 1))
+UNIT, LAG, LEAD = 7.73, 2.0, 16.0
+
+
+def crossing(src, p, n_z):
+    return PARTS[p][0] == "down" and 2 * src >= n_z
+
+
+def sort_of(src, p, n_z):
+    return "a" if crossing(src, p, n_z) else PARTS[p][3]
+
+
+def length(p):
+    return UNIT * (0.5 if PARTS[p][0] == "down" else PARTS[p][2] / 8)
+
+
+def rank(n_z, m, link, item):
+    src, side, p = item
+    if link == "x":
+        return (0,)
+    b = sort_of(src, p, n_z) == "b"
+    if link == "y" and b:
+        return (0, p)
+    if PARTS[p][0] == "down":
+        return (1 if crossing(src, p, n_z) else 4, p, abs(src - m), side)
+    return (3 if b else 2, p, abs(src - m), side)
+
+
+def simulate(n_z):
+    queue, free, sent = {}, {}, {}
+    events, have = [], [{} for _ in range(n_z)]
+    far_in = [{} for _ in range(n_z)]
+    count = [0]
+    for m in range(n_z):
+        for link in ("up", "dn", "y", "x"):
+            queue[m, link], free[m, link], sent[m, link] = [], True, []
+
+    def add(at, what, *rest):
+        count[0] += 1
+        heapq.heappush(events, (at, count[0], what, rest))
+
+    def kick(at, m, link):
+        if free[m, link] and queue[m, link]:
+            queue[m, link].sort()
+            _, item = queue[m, link].pop(0)
+            free[m, link] = False
+            sent[m, link].append((at, item))
+            add(at + length(item[2]), "free", m, link)
+            add(at + length(item[2]) + LAG, "land", m, link, item)
+
+    def put(at, m, link, item):
+        queue[m, link].append((rank(n_z, m, link, item), item))
+        kick(at, m, link)
+
+    def got(at, m, item):
+        src, side, p = item
+        have[m][item] = at
+        b = sort_of(src, p, n_z) == "b"
+        if side == 0 or b:
+            if m >= src and m < n_z - 1:
+                put(at, m, "up", item)
+            if m <= src and m > 0:
+                put(at, m, "dn", item)
+        if side == 0 and (not b or m == src):
+            put(at, m, "y", item)
+        if crossing(src, p, n_z):
+            put(at, m, "x", item)
+
+    for m in range(n_z):
+        for p in range(len(PARTS)):
+            add(0.0, "own", m, (m, 0, p))
+    while events:
+        at, _, what, rest = heapq.heappop(events)
+        if what == "own":
+            got(at, *rest)
+        elif what == "free":
+            free[rest] = True
+            kick(at, *rest)
+        else:
+            m, link, item = rest
+            if link == "x":
+                far_in[n_z - 1 - m][item] = at
+            elif link == "y":
+                got(at, m, (item[0], 1, item[2]))
+            else:
+                got(at, m + (1 if link == "up" else -1), item)
+    return have, far_in, sent
+
+
+def timetable(n_z):
+    have, far_in, sent = simulate(n_z)
+    sources, ready = {}, {}
+    for m in range(n_z):
+        for name in ("gate", "up"):
+            mine = [p for p in range(len(PARTS)) if PARTS[p][0] == name]
+            done = sorted((max(have[m][src, side, p] for side in (0, 1) for p in mine), src) for src in range(n_z))
+            for j, (at, src) in enumerate(done):
+                sources[m, name, j], ready[m, (name, j)] = src, at
+        ready[m, ("norm", 0)] = 1.0
+        ready[m, ("act", 0)] = 0.0
+        for g, (q, n) in enumerate(FAR_GROUPS):
+            ready[m, ("far", g)] = max(at for item, at in far_in[m].items() if q <= PARTS[item[2]][1] < q + n)
+        for g, (q, n) in enumerate(NEAR_GROUPS):
+            ready[m, ("near", g)] = 2.0 + max(
+                at for item, at in have[m].items()
+                if PARTS[item[2]][0] == "down" and not crossing(item[0], item[2], n_z) and q <= PARTS[item[2]][1] < q + n
+            )
+        ready[m, ("end", 0)] = 1e9
+    muls = sorted(
+        (sum(ready[m, (name, j)] for m in range(n_z)), name, j) for name in ("gate", "up") for j in range(n_z)
+    )
+    steps = [("norm", 0)] + [(name, j) for _, name, j in muls] + [("act", 0)]
+    steps += [("far", g) for g in range(len(FAR_GROUPS))] + [("near", g) for g in range(len(NEAR_GROUPS))] + [("end", 0)]
+    spans = {"norm": 3.0, "gate": 1.5, "up": 1.5, "act": 1.5, "far": 3.0, "near": 1.0, "end": 0.0}
+    before = {}
+    for m in range(n_z):
+        todo = [(at, 0, "wait", item) for item, at in have[m].items() if at > 0.0]
+        for link in ("up", "dn", "y", "x"):
+            last = 0.0
+            for at, item in sent[m, link]:
+                last = max(last, have[m][item], at - LEAD)
+                todo.append((last, 1, link, item))
+        for item, at in have[m].items():
+            if PARTS[item[2]][0] == "down" and not crossing(item[0], item[2], n_z):
+                todo.append((at, 1, "core", item))
+        todo.sort(key=lambda e: e[:2])
+        now = 0.0
+        for step in steps:
+            now = max(now, ready[m, step])
+            before[m, step] = [e[2:] for e in todo if e[0] <= now]
+            todo = [e for e in todo if e[0] > now]
+            now += spans[step[0]]
+    return steps, sources, before
+
+
+def line_kernel(
+    n_fs, n_tp, tok_hbm, gain, gw, uw, dw, gate_o, up_o, down_o, mix_o,
+    tok, dcol, normed, acc_g, acc_u, hidden, far_a, far_b, far_in, out_send, out_in, near_sh, near_in, own_sh,
+    tok_sem, ag_send, ag_recv, aa_send, aa_recv, fp_send, fp_recv, ac_send, ac_recv, np_send, np_recv,
+):
+    tok_copy = pltpu.make_async_copy(tok_hbm, tok, tok_sem)
+    tok_copy.start()
+    f, t = lax.axis_index("fs"), lax.axis_index("tp")
+    n_z = n_fs // 2
+    z, y = f // 2, f % 2
+    x = t // 2
+    per = n_fs // n_tp
+    rows = gw.shape[0]
+    d_rows, d_cols = dw.shape
+    part = d_cols // 4
+    n_tok = tok.shape[0]
+    k_z = normed.shape[2]
+    m_tile = min(256, n_tok)
+    width = gw.shape[1]
+    col_tiles = [(c, min(512, width - c)) for c in range(0, width, 512)]
+    place = z + x * (n_z - 1 - 2 * z)
+    ahead = f + 2 - 4 * x
+    behind = f - 2 + 4 * x
+    other_y = f + 1 - 2 * y
+    near = t + 1 - 2 * (t % 2)
+    far = t + 2 - 4 * x
+    far_near = far + 1 - 2 * (far % 2)
+    steps, sources, before = timetable(n_z)
+
+    def z_of(src):
+        return src + x * (n_z - 1 - 2 * src)
+
+    def owner_of(item):
+        src, side, _ = item
+        return 2 * z_of(src) + (y if side == 0 else 1 - y)
+
+    def view(o, p):
+        name, first, n, _ = PARTS[p]
+        if name == "down":
+            return dcol.at[o, :, pl.ds(first * part, n * part)]
+        ref = gate_o if name == "gate" else up_o
+        step = rows // 16
+        return ref.at[pl.ds(pl.multiple_of(o * rows + first * step, step), n * step), :]
+
+    def ag(item, way, dest):
+        o, p = owner_of(item), item[2]
+        v = view(o, p)
+        return pltpu.make_async_remote_copy(
+            v, v, ag_send.at[o, p, way], ag_recv.at[o, p], device_id=(dest, t), device_id_type=MESH,
+        )
+
+    def hand(item):
+        o, p = owner_of(item), item[2]
+        _, first, n, _ = PARTS[p]
+        row = pl.multiple_of((o % per) * d_rows, d_rows)
+        col = pl.multiple_of(t * d_cols + first * part, part)
+        return pltpu.make_async_remote_copy(
+            view(o, p), down_o.at[pl.ds(row, d_rows), pl.ds(col, n * part)],
+            aa_send.at[o, p], aa_recv.at[t, o % per, p],
+            device_id=(f, o // per), device_id_type=MESH,
+        )
+
+    def transfer(what, item):
+        if what == "up":
+            return ag(item, 0, ahead)
+        if what == "dn":
+            return ag(item, 1, behind)
+        if what == "y":
+            return ag(item, 2, other_y)
+        return hand(item)
+
+    def elsewhere(item):
+        return owner_of(item) // per != t
+
+    def play(step):
+        for m in range(n_z):
+            def events(m=m):
+                for what, item in before[m, step]:
+                    if what == "wait":
+                        ag(item, 0, f).wait_recv()
+                    elif what == "core":
+                        pl.when(elsewhere(item))(lambda item=item: hand(item).start())
+                    else:
+                        transfer(what, item).start()
+            if before[m, step]:
+                pl.when(place == m)(events)
+
+    barrier = pltpu.get_barrier_semaphore()
+    peers = [
+        (z > 0, (f - 2, t)), (z < n_z - 1, (f + 2, t)), (None, (other_y, t)),
+        (None, (f, near)), (None, (f, far)), (None, (f, far_near)),
+    ]
+    for cond, dev in peers:
+        def hello(dev=dev):
+            pl.semaphore_signal(barrier, inc=1, device_id=dev, device_id_type=MESH)
+        hello() if cond is None else pl.when(cond)(hello)
+
+    g = jnp.broadcast_to(gain[...], (8, rows)).T[:, :1]
+    base = pl.multiple_of(f * rows, rows)
+    gate_o[pl.ds(base, rows), :] = (gw[...] * g).astype(jnp.bfloat16)
+    dcol[f] = dw[...].astype(jnp.bfloat16)
+    up_o[pl.ds(base, rows), :] = (uw[...] * g).astype(jnp.bfloat16)
+    inner = jnp.logical_and(z > 0, z < n_z - 1)
+    pl.when(inner)(lambda: pl.semaphore_wait(barrier, len(peers)))
+    pl.when(jnp.logical_not(inner))(lambda: pl.semaphore_wait(barrier, len(peers) - 1))
+
+    def norm():
+        tok_copy.wait()
+
+        @pl.loop(0, n_tok // 64)
+        def _(i):
+            r = pl.multiple_of(i * 64, 64)
+            v = tok[pl.ds(r, 64), :].astype(jnp.float32)
+            v = v * lax.rsqrt(jnp.mean(v * v, axis=-1, keepdims=True) + eps_norm)
+            v = v.astype(jnp.bfloat16)
+            for j in range(n_z):
+                normed[j, pl.ds(r, 64), :] = v[:, j * k_z : (j + 1) * k_z]
+
+    def multiply(w, acc, src, first):
+        zz = z_of(src)
+        k0 = pl.multiple_of(zz * k_z, k_z)
+
+        @pl.loop(0, n_tok // m_tile)
+        def _(i):
+            r = pl.multiple_of(i * m_tile, m_tile)
+            a = normed[zz, pl.ds(r, m_tile), :]
+            for c, n in col_tiles:
+                v = jnp.dot(a, w[pl.ds(k0, k_z), c : c + n], preferred_element_type=jnp.float32)
+                if first:
+                    acc[pl.ds(r, m_tile), c : c + n] = v
+                else:
+                    acc[pl.ds(r, m_tile), c : c + n] += v
+
+    def act():
+        @pl.loop(0, n_tok // 32)
+        def _(i):
+            r = pl.multiple_of(i * 32, 32)
+            v = acc_g[pl.ds(r, 32), :]
+            hidden[pl.ds(r, 32), :] = (v / (1.0 + jnp.exp(-v)) * acc_u[pl.ds(r, 32), :]).astype(jnp.bfloat16)
+
+    def arrived(c, q, n):
+        for k in range(per):
+            for p in DOWN:
+                _, first, m, _ = PARTS[p]
+                if q <= first < q + n:
+                    ref = down_o.at[
+                        pl.ds(k * d_rows, d_rows), pl.ds(pl.multiple_of(c * d_cols + first * part, part), m * part)
+                    ]
+                    pltpu.make_async_remote_copy(
+                        ref, ref, aa_send.at[0, p], aa_recv.at[c, k, p], device_id=(f, near), device_id_type=MESH,
+                    ).wait_recv()
+
+    def product(c, q, n, out):
+        @pl.loop(0, n_tok // m_tile)
+        def _(i):
+            r = pl.multiple_of(i * m_tile, m_tile)
+            col = pl.multiple_of(c * d_cols + q * part, part)
+            v = jnp.dot(
+                hidden[pl.ds(r, m_tile), :], down_o[:, pl.ds(col, n * part)], preferred_element_type=jnp.float32
+            )
+            out[pl.ds(r, m_tile), :] = v.astype(jnp.bfloat16)
+
+    def cols(q, n):
+        return slice(q * part, (q + n) * part)
+
+    def far_pair(i):
+        q, n = FAR_GROUPS[i]
+        return pltpu.make_async_remote_copy(
+            far_a.at[:, cols(q, n)], far_in.at[:, cols(q, n)], fp_send.at[i], fp_recv.at[i],
+            device_id=(f, near), device_id_type=MESH,
+        )
+
+    def across(i):
+        q, n = FAR_GROUPS[i]
+        return pltpu.make_async_remote_copy(
+            out_send.at[:, cols(q, n)], out_in.at[:, cols(q, n)], ac_send.at[i], ac_recv.at[i],
+            device_id=(f, far), device_id_type=MESH,
+        )
+
+    def near_pair(i):
+        q, n = NEAR_GROUPS[i]
+        return pltpu.make_async_remote_copy(
+            near_sh.at[:, cols(q, n)], near_in.at[:, cols(q, n)], np_send.at[i], np_recv.at[i],
+            device_id=(f, near), device_id_type=MESH,
+        )
+
+    def far_step(i):
+        q, n = FAR_GROUPS[i]
+        arrived(far_near, q, n)
+        product(far_near, q, n, far_a.at[:, cols(q, n)])
+        far_pair(i).start()
+        arrived(far, q, n)
+        product(far, q, n, far_b.at[:, cols(q, n)])
+        far_pair(i).wait_recv()
+        out_send[:, cols(q, n)] = (
+            far_b[:, cols(q, n)].astype(jnp.float32) + far_in[:, cols(q, n)].astype(jnp.float32)
+        ).astype(jnp.bfloat16)
+        across(i).start()
+
+    def near_step(i):
+        q, n = NEAR_GROUPS[i]
+        col = pl.multiple_of(t * d_cols + q * part, part)
+        for k in range(per):
+            down_o[k * d_rows : (k + 1) * d_rows, pl.ds(col, n * part)] = dcol[t * per + k, :, cols(q, n)]
+        arrived(near, q, n)
+        product(near, q, n, near_sh.at[:, cols(q, n)])
+        near_pair(i).start()
+        product(t, q, n, own_sh.at[:, cols(q, n)])
+
+    def end():
+        for i in range(len(FAR_GROUPS)):
+            across(i).wait_recv()
+        for i, (q, n) in enumerate(NEAR_GROUPS):
+            near_pair(i).wait_recv()
+            c = cols(q, n)
+            mix_o[:, c] = (
+                own_sh[:, c].astype(jnp.float32) + near_in[:, c].astype(jnp.float32) + out_in[:, c].astype(jnp.float32)
+            ).astype(jnp.bfloat16)
+
+    done = {"gate": 0, "up": 0}
+    for step in steps:
+        play(step)
+        what, i = step
+        if what == "norm":
+            norm()
+        elif what == "act":
+            act()
+        elif what == "far":
+            far_step(i)
+        elif what == "near":
+            near_step(i)
+        elif what == "end":
+            end()
+        else:
+            src = sources[0, what, i]
+            for m in range(1, n_z):
+                src = jnp.where(place == m, sources[m, what, i], src)
+            multiply(gate_o if what == "gate" else up_o, acc_g if what == "gate" else acc_u, src, done[what] == 0)
+            done[what] += 1
+
+    for i in range(len(FAR_GROUPS)):
+        far_pair(i).wait_send()
+        across(i).wait_send()
+    for i in range(len(NEAR_GROUPS)):
+        near_pair(i).wait_send()
+    for m in range(n_z):
+        @pl.when(place == m)
+        def _(m=m):
+            for step in steps:
+                for what, item in before[m, step]:
+                    if what == "core":
+                        pl.when(elsewhere(item))(lambda item=item: hand(item).wait_send())
+                    elif what != "wait":
+                        transfer(what, item).wait_send()
+
+
+def line_on_device(n_fs, n_tp, tokens, norm_gain, gate_weight, up_weight, down_weight):
+    n_tok, d_model = tokens.shape
+    rows, width = gate_weight.shape
+    d_rows, d_cols = down_weight.shape
+    n_z = n_fs // 2
+    n_p = len(PARTS)
+    bf = jnp.bfloat16
+    vmem = pl.BlockSpec(memory_space=pltpu.VMEM)
+    dma = pltpu.SemaphoreType.DMA
+    n_far, n_near = len(FAR_GROUPS), len(NEAR_GROUPS)
+    return pl.pallas_call(
+        functools.partial(line_kernel, n_fs, n_tp),
+        out_shape=(
+            pltpu.VMEM((d_model, width), bf),
+            pltpu.VMEM((d_model, width), bf),
+            pltpu.VMEM((d_rows * n_fs // n_tp, d_model), bf),
+            pltpu.VMEM((n_tok, d_cols), bf),
+        ),
+        in_specs=[pl.BlockSpec(memory_space=pl.ANY)] + [vmem] * 4,
+        out_specs=(vmem,) * 4,
+        scratch_shapes=[
+            pltpu.VMEM((n_tok, d_model), bf),
+            pltpu.VMEM((n_fs, d_rows, d_cols), bf),
+            pltpu.VMEM((n_z, n_tok, d_model // n_z), bf),
+            pltpu.VMEM((n_tok, width), jnp.float32),
+            pltpu.VMEM((n_tok, width), jnp.float32),
+            pltpu.VMEM((n_tok, width), bf),
+            *[pltpu.VMEM((n_tok, d_cols), bf)] * 8,
+            dma,
+            dma((n_fs, n_p, 3)),
+            dma((n_fs, n_p)),
+            dma((n_fs, n_p)),
+            dma((n_tp, n_fs // n_tp, n_p)),
+            dma((n_far,)),
+            dma((n_far,)),
+            dma((n_far,)),
+            dma((n_far,)),
+            dma((n_near,)),
+            dma((n_near,)),
+        ],
+        compiler_params=pltpu.CompilerParams(
+            collective_id=0, has_side_effects=True, vmem_limit_bytes=46 * 2**20
+        ),
+    )(tokens, norm_gain[None, :], gate_weight, up_weight, down_weight)
+
+
 def solution(mesh):
     n_fs, n_tp = mesh.shape["fs"], mesh.shape["tp"]
     in_specs = (P("fs", None), P("fs"), P("fs", "tp"), P("fs", "tp"), P("fs", "tp"))
     out_specs = (P(None, "tp"), P(None, "tp"), P("tp", None), P("fs", "tp"))
+    body = line_on_device if (n_fs, n_tp) == (8, 4) else on_device
     return jax.shard_map(
-        functools.partial(on_device, n_fs, n_tp), mesh=mesh, in_specs=in_specs, out_specs=out_specs, check_vma=False
+        functools.partial(body, n_fs, n_tp), mesh=mesh, in_specs=in_specs, out_specs=out_specs, check_vma=False
     )

time: 216 us -> 194 us (0.90)
  Pallas kernels: 207 us -> 185 us
    pallas_call x1, Pallas kernels: 207 us -> 185 us  [line_on_device(): pl.pallas_call(functools.partial(line_kernel, n_fs, n_tp), out_shape=(plt...]
where the time goes in v1:
time: 194 us
  Pallas kernels  185 us (95%)
  local copies, waits for them, and re-layouts  8.47 us (4%)
    pallas_call x1, Pallas kernels, line_on_device(): pl.pallas_call(functools.partial(line_kernel, n_fs, n_tp), out_shape=(plt...  185 us
    unnamed x4, local copies, waits for them, and re-layouts  8.47 us

profile of v1, /device:TPU:0, one launch (start us, length us, event | category | flops | bytes accessed | tf_op | source)
XLA Modules:
  0.0 193.9 jit_solution(18344183942785242556)
XLA Ops:
  0.6 184.8 %shard_map.84 = (bf16[2048,1408]{1,0:T(8,128)(2,1)S(1)}, bf16[2048,1408]{1,0:T(8,128)(2,1)S(1)}, bf16[1408,2048]{1,0:T(8,128)(2,1)S(1)}, bf16[768,512]{1,0:T(8,128)(2,1)S(1)}) custom-call(bf16[768,2048]{1,0:T(8,128)(2,1)} %tok_hbm.1, f32[1,256]{1,0:T(1,128)} %bitcast.1, f32[256,1408]{1,0:T(8,128)} %gw.1, f32[256,1408]{1,0:T(8,128)} %uw.1, f32[704,512]{1,0:T(8,128)} %dw.1), custom_call_target="tpu_custom_call" | custom-call | tf_op jit(solution)/shard_map/pallas_call | solution.py:808
  185.4 2.5 %copy.13 = bf16[2048,1408]{1,0:T(8,128)(2,1)} copy(bf16[2048,1408]{1,0:T(8,128)(2,1)S(1)} %get-tuple-element.4) | data formatting | bytes 11534336
  187.9 0.9 copy.16
  188.8 2.5 %copy.14 = bf16[2048,1408]{1,0:T(8,128)(2,1)} copy(bf16[2048,1408]{1,0:T(8,128)(2,1)S(1)} %get-tuple-element.5) | data formatting | bytes 11534336
  191.3 2.5 %copy.15 = bf16[1408,2048]{1,0:T(8,128)(2,1)} copy(bf16[1408,2048]{1,0:T(8,128)(2,1)S(1)} %get-tuple-element.6) | data formatting | bytes 11534336

commit v2 on v1

--- a/solution.py
+++ b/solution.py
@@ -412,8 +412,10 @@
     return PARTS[p][0] == "down" and 2 * src >= n_z
 
 
-def sort_of(src, p, n_z):
-    return "a" if crossing(src, p, n_z) else PARTS[p][3]
+def reach(src, p, n_z):
+    if crossing(src, p, n_z) or PARTS[p][3] == "a":
+        return (src, src)
+    return (0, n_z - 1)
 
 
 def length(p):
@@ -424,7 +426,7 @@
     src, side, p = item
     if link == "x":
         return (0,)
-    b = sort_of(src, p, n_z) == "b"
+    b = reach(src, p, n_z) != (src, src)
     if link == "y" and b:
         return (0, p)
     if PARTS[p][0] == "down":
@@ -461,20 +463,19 @@
     def got(at, m, item):
         src, side, p = item
         have[m][item] = at
-        b = sort_of(src, p, n_z) == "b"
-        if side == 0 or b:
-            if m >= src and m < n_z - 1:
-                put(at, m, "up", item)
-            if m <= src and m > 0:
-                put(at, m, "dn", item)
-        if side == 0 and (not b or m == src):
+        low, high = reach(src, p, n_z)
+        if m >= src and m < (n_z - 1 if side == 0 else high):
+            put(at, m, "up", item)
+        if m <= src and m > (0 if side == 0 else low):
+            put(at, m, "dn", item)
+        if side == 0 and (m == src or not low <= m <= high):
             put(at, m, "y", item)
         if crossing(src, p, n_z):
             put(at, m, "x", item)
 
     for m in range(n_z):
         for p in range(len(PARTS)):
-            add(0.0, "own", m, (m, 0, p))
+            add(1.0 if PARTS[p][0] == "up" else 0.0, "own", m, (m, 0, p))
     while events:
         at, _, what, rest = heapq.heappop(events)
         if what == "own":
@@ -502,12 +503,13 @@
             done = sorted((max(have[m][src, side, p] for side in (0, 1) for p in mine), src) for src in range(n_z))
             for j, (at, src) in enumerate(done):
                 sources[m, name, j], ready[m, (name, j)] = src, at
-        ready[m, ("norm", 0)] = 1.0
+        ready[m, ("lift", 0)] = 0.5
+        ready[m, ("norm", 0)] = 1.5
         ready[m, ("act", 0)] = 0.0
         for g, (q, n) in enumerate(FAR_GROUPS):
             ready[m, ("far", g)] = max(at for item, at in far_in[m].items() if q <= PARTS[item[2]][1] < q + n)
         for g, (q, n) in enumerate(NEAR_GROUPS):
-            ready[m, ("near", g)] = 2.0 + max(
+            ready[m, ("near", g)] = max(
                 at for item, at in have[m].items()
                 if PARTS[item[2]][0] == "down" and not crossing(item[0], item[2], n_z) and q <= PARTS[item[2]][1] < q + n
             )
@@ -515,12 +517,12 @@
     muls = sorted(
         (sum(ready[m, (name, j)] for m in range(n_z)), name, j) for name in ("gate", "up") for j in range(n_z)
     )
-    steps = [("norm", 0)] + [(name, j) for _, name, j in muls] + [("act", 0)]
+    steps = [("lift", 0), ("norm", 0)] + [(name, j) for _, name, j in muls] + [("act", 0)]
     steps += [("far", g) for g in range(len(FAR_GROUPS))] + [("near", g) for g in range(len(NEAR_GROUPS))] + [("end", 0)]
-    spans = {"norm": 3.0, "gate": 1.5, "up": 1.5, "act": 1.5, "far": 3.0, "near": 1.0, "end": 0.0}
+    spans = {"lift": 0.5, "norm": 3.0, "gate": 1.5, "up": 1.5, "act": 1.5, "far": 3.0, "near": 0.2, "end": 0.0}
     before = {}
     for m in range(n_z):
-        todo = [(at, 0, "wait", item) for item, at in have[m].items() if at > 0.0]
+        todo = [(at, 0, "wait", item) for item, at in have[m].items() if item[:2] != (m, 0)]
         for link in ("up", "dn", "y", "x"):
             last = 0.0
             for at, item in sent[m, link]:
@@ -540,12 +542,16 @@
 
 
 def line_kernel(
-    n_fs, n_tp, tok_hbm, gain, gw, uw, dw, gate_o, up_o, down_o, mix_o,
-    tok, dcol, normed, acc_g, acc_u, hidden, far_a, far_b, far_in, out_send, out_in, near_sh, near_in, own_sh,
-    tok_sem, ag_send, ag_recv, aa_send, aa_recv, fp_send, fp_recv, ac_send, ac_recv, np_send, np_recv,
+    n_fs, n_tp, tok_hbm, gain, gw_hbm, uw_hbm, dw_hbm, gate_o, up_o, down_o, dcol, hidden, hidden_near, out_in,
+    tok, gw, uw, dw, normed, acc_g, acc_u, far_a, far_b, far_in, out_send,
+    in_sem, ag_send, ag_recv, aa_send, aa_recv, fp_send, fp_recv, ac_send, ac_recv, hid_send, hid_recv,
 ):
-    tok_copy = pltpu.make_async_copy(tok_hbm, tok, tok_sem)
-    tok_copy.start()
+    loads = [
+        pltpu.make_async_copy(src, dst, in_sem.at[i])
+        for i, (src, dst) in enumerate(((gw_hbm, gw), (dw_hbm, dw), (uw_hbm, uw), (tok_hbm, tok)))
+    ]
+    for load in loads:
+        load.start()
     f, t = lax.axis_index("fs"), lax.axis_index("tp")
     n_z = n_fs // 2
     z, y = f // 2, f % 2
@@ -638,15 +644,20 @@
 
     g = jnp.broadcast_to(gain[...], (8, rows)).T[:, :1]
     base = pl.multiple_of(f * rows, rows)
+    loads[0].wait()
     gate_o[pl.ds(base, rows), :] = (gw[...] * g).astype(jnp.bfloat16)
+    loads[1].wait()
     dcol[f] = dw[...].astype(jnp.bfloat16)
-    up_o[pl.ds(base, rows), :] = (uw[...] * g).astype(jnp.bfloat16)
     inner = jnp.logical_and(z > 0, z < n_z - 1)
     pl.when(inner)(lambda: pl.semaphore_wait(barrier, len(peers)))
     pl.when(jnp.logical_not(inner))(lambda: pl.semaphore_wait(barrier, len(peers) - 1))
 
+    def lift():
+        loads[2].wait()
+        up_o[pl.ds(base, rows), :] = (uw[...] * g).astype(jnp.bfloat16)
+
     def norm():
-        tok_copy.wait()
+        loads[3].wait()
 
         @pl.loop(0, n_tok // 64)
         def _(i):
@@ -718,11 +729,9 @@
             device_id=(f, far), device_id_type=MESH,
         )
 
-    def near_pair(i):
-        q, n = NEAR_GROUPS[i]
+    def hidden_copy():
         return pltpu.make_async_remote_copy(
-            near_sh.at[:, cols(q, n)], near_in.at[:, cols(q, n)], np_send.at[i], np_recv.at[i],
-            device_id=(f, near), device_id_type=MESH,
+            hidden, hidden_near, hid_send, hid_recv, device_id=(f, near), device_id_type=MESH,
         )
 
     def far_step(i):
@@ -743,29 +752,24 @@
         col = pl.multiple_of(t * d_cols + q * part, part)
         for k in range(per):
             down_o[k * d_rows : (k + 1) * d_rows, pl.ds(col, n * part)] = dcol[t * per + k, :, cols(q, n)]
-        arrived(near, q, n)
-        product(near, q, n, near_sh.at[:, cols(q, n)])
-        near_pair(i).start()
-        product(t, q, n, own_sh.at[:, cols(q, n)])
 
     def end():
+        arrived(near, 0, 4)
         for i in range(len(FAR_GROUPS)):
             across(i).wait_recv()
-        for i, (q, n) in enumerate(NEAR_GROUPS):
-            near_pair(i).wait_recv()
-            c = cols(q, n)
-            mix_o[:, c] = (
-                own_sh[:, c].astype(jnp.float32) + near_in[:, c].astype(jnp.float32) + out_in[:, c].astype(jnp.float32)
-            ).astype(jnp.bfloat16)
+        hidden_copy().wait_recv()
 
     done = {"gate": 0, "up": 0}
     for step in steps:
         play(step)
         what, i = step
-        if what == "norm":
+        if what == "lift":
+            lift()
+        elif what == "norm":
             norm()
         elif what == "act":
             act()
+            hidden_copy().start()
         elif what == "far":
             far_step(i)
         elif what == "near":
@@ -782,8 +786,7 @@
     for i in range(len(FAR_GROUPS)):
         far_pair(i).wait_send()
         across(i).wait_send()
-    for i in range(len(NEAR_GROUPS)):
-        near_pair(i).wait_send()
+    hidden_copy().wait_send()
     for m in range(n_z):
         @pl.when(place == m)
         def _(m=m):
@@ -795,6 +798,38 @@
                         transfer(what, item).wait_send()
 
 
+def finish(
+    n_tp, gate_i, up_i, down_i, dcol, hidden, hidden_near, out_in, gate_o, up_o, down_o, mix_o, near_w, mix, sems,
+):
+    t = lax.axis_index("tp")
+    near = t + 1 - 2 * (t % 2)
+    per = dcol.shape[0] // n_tp
+    d_rows, d_cols = dcol.shape[1:]
+    n_tok = hidden.shape[0]
+    m_tile = min(256, n_tok)
+    copies = [
+        pltpu.make_async_copy(src, dst, sems.at[i])
+        for i, (src, dst) in enumerate(((gate_i, gate_o), (up_i, up_o), (down_i, down_o), (mix, mix_o)))
+    ]
+    for copy in copies[:3]:
+        copy.start()
+    for k in range(per):
+        near_w[k * d_rows : (k + 1) * d_rows, :] = dcol[near * per + k]
+    col = pl.multiple_of(t * d_cols, d_cols)
+
+    @pl.loop(0, n_tok // m_tile)
+    def _(i):
+        r = pl.ds(pl.multiple_of(i * m_tile, m_tile), m_tile)
+        own = jnp.dot(hidden[r, :], down_i[:, pl.ds(col, d_cols)], preferred_element_type=jnp.float32)
+        other = jnp.dot(hidden_near[r, :], near_w[...], preferred_element_type=jnp.float32)
+        own, other = own.astype(jnp.bfloat16).astype(jnp.float32), other.astype(jnp.bfloat16).astype(jnp.float32)
+        mix[r, :] = (own + other + out_in[r, :].astype(jnp.float32)).astype(jnp.bfloat16)
+
+    copies[3].start()
+    for copy in copies:
+        copy.wait()
+
+
 def line_on_device(n_fs, n_tp, tokens, norm_gain, gate_weight, up_weight, down_weight):
     n_tok, d_model = tokens.shape
     rows, width = gate_weight.shape
@@ -804,26 +839,28 @@
     bf = jnp.bfloat16
     vmem = pl.BlockSpec(memory_space=pltpu.VMEM)
     dma = pltpu.SemaphoreType.DMA
-    n_far, n_near = len(FAR_GROUPS), len(NEAR_GROUPS)
-    return pl.pallas_call(
+    n_far = len(FAR_GROUPS)
+    hbm = pl.BlockSpec(memory_space=pl.ANY)
+    d_own = d_rows * n_fs // n_tp
+    shapes = (
+        (d_model, width), (d_model, width), (d_own, d_model), (n_fs, d_rows, d_cols),
+        (n_tok, width), (n_tok, width), (n_tok, d_cols),
+    )
+    held = pl.pallas_call(
         functools.partial(line_kernel, n_fs, n_tp),
-        out_shape=(
-            pltpu.VMEM((d_model, width), bf),
-            pltpu.VMEM((d_model, width), bf),
-            pltpu.VMEM((d_rows * n_fs // n_tp, d_model), bf),
-            pltpu.VMEM((n_tok, d_cols), bf),
-        ),
-        in_specs=[pl.BlockSpec(memory_space=pl.ANY)] + [vmem] * 4,
-        out_specs=(vmem,) * 4,
+        out_shape=tuple(pltpu.VMEM(shape, bf) for shape in shapes),
+        in_specs=[hbm, vmem, hbm, hbm, hbm],
+        out_specs=(vmem,) * len(shapes),
         scratch_shapes=[
             pltpu.VMEM((n_tok, d_model), bf),
-            pltpu.VMEM((n_fs, d_rows, d_cols), bf),
+            pltpu.VMEM((rows, width), jnp.float32),
+            pltpu.VMEM((rows, width), jnp.float32),
+            pltpu.VMEM((d_rows, d_cols), jnp.float32),
             pltpu.VMEM((n_z, n_tok, d_model // n_z), bf),
             pltpu.VMEM((n_tok, width), jnp.float32),
             pltpu.VMEM((n_tok, width), jnp.float32),
-            pltpu.VMEM((n_tok, width), bf),
-            *[pltpu.VMEM((n_tok, d_cols), bf)] * 8,
-            dma,
+            *[pltpu.VMEM((n_tok, d_cols), bf)] * 4,
+            dma((4,)),
             dma((n_fs, n_p, 3)),
             dma((n_fs, n_p)),
             dma((n_fs, n_p)),
@@ -832,13 +869,24 @@
             dma((n_far,)),
             dma((n_far,)),
             dma((n_far,)),
-            dma((n_near,)),
-            dma((n_near,)),
+            dma,
+            dma,
         ],
         compiler_params=pltpu.CompilerParams(
-            collective_id=0, has_side_effects=True, vmem_limit_bytes=46 * 2**20
+            collective_id=0, has_side_effects=True, vmem_limit_bytes=30 * 2**20
         ),
     )(tokens, norm_gain[None, :], gate_weight, up_weight, down_weight)
+    return pl.pallas_call(
+        functools.partial(finish, n_tp),
+        out_shape=tuple(
+            jax.ShapeDtypeStruct(shape, bf)
+            for shape in ((d_model, width), (d_model, width), (d_own, d_model), (n_tok, d_cols))
+        ),
+        in_specs=[vmem] * len(shapes),
+        out_specs=(hbm,) * 4,
+        scratch_shapes=[pltpu.VMEM((d_own, d_cols), bf), pltpu.VMEM((n_tok, d_cols), bf), dma((4,))],
+        compiler_params=pltpu.CompilerParams(vmem_limit_bytes=6 * 2**20),
+    )(*held)
 
 
 def solution(mesh):

time: 194 us -> 187 us (0.964)
  local copies, waits for them, and re-layouts: 8.47 us -> 0 us
    unnamed x4 -> x0, local copies, waits for them, and re-layouts: 8.47 us -> none
    pallas_call x1 -> x2, Pallas kernels: 185 us -> 185 us  [the longest x1 178 us: line_on_device(): pl.pallas_call(functools.partial(line_kernel, n_fs, n_tp), out_shape=tupl...]
where the time goes in v2:
time: 187 us; the launch traced here: 185 us
  Pallas kernels  185 us (99%)
    pallas_call x1, Pallas kernels, line_on_device(): pl.pallas_call(functools.partial(line_kernel, n_fs, n_tp), out_shape=tupl...  178 us
    pallas_call x1, Pallas kernels, line_on_device(): pl.pallas_call(functools.partial(finish, n_tp), out_shape=tuple((jax.Shap...  6.28 us

profile of v2, /device:TPU:0, one launch (start us, length us, event | category | flops | bytes accessed | tf_op | source)
XLA Modules:
  0.0 185.2 jit_solution(9742270145547795187)
XLA Ops:
  0.6 178.3 %shard_map.84 = (bf16[2048,1408]{1,0:T(8,128)(2,1)S(1)}, bf16[2048,1408]{1,0:T(8,128)(2,1)S(1)}, bf16[1408,2048]{1,0:T(8,128)(2,1)S(1)}, bf16[8,704,512]{2,1,0:T...) custom-call(bf16[768,2048]{1,0:T(8,128)(2,1)} %tok_hbm.1, ...), custom_call_target="tpu_custom_call" | custom-call | tf_op jit(solution)/shard_map/pallas_call | solution.py:849
  179.0 6.3 %shard_map.85 = (bf16[2048,1408]{1,0:T(8,128)(2,1)}, bf16[2048,1408]{1,0:T(8,128)(2,1)}, bf16[1408,2048]{1,0:T(8,128)(2,1)}, bf16[768,512]{1,0:T(8,128)(2,1)}) custom-call(bf16[2048,1408]{1,0:T(8,128)(2,1)S(1)} %get-tuple-element.11.gate_i, bf16[2048,1408]{1,0:T(8,128)(2,1)S(1)} %get-tuple-element.12.up_i, bf16[1408,2048]{1,0:T(8,128)(2,1)S(1)} %get-tuple-element.13.down_i, ...), custom_call_target="tpu_custom_call" | custom-call | tf_op jit(solution)/shard_map/pallas_call | solution.py:879

commit v3 on v2

--- a/solution.py
+++ b/solution.py
@@ -392,46 +392,56 @@
 
 
 PARTS = (
-    ("gate", 0, 8, "a"),
-    ("gate", 8, 8, "a"),
-    ("up", 0, 6, "a"),
-    ("up", 6, 5, "a"),
-    ("up", 11, 5, "b"),
-    ("down", 0, 1, "a"),
-    ("down", 1, 1, "a"),
-    ("down", 2, 1, "a"),
-    ("down", 3, 1, "b"),
+    ("gate", 0, 8),
+    ("gate", 8, 8),
+    ("up", 0, 8),
+    ("up", 8, 4),
+    ("up", 12, 4),
+    ("down", 0, 1),
+    ("down", 1, 1),
+    ("down", 2, 1),
+    ("down", 3, 1),
 )
+REACH = (
+    ((0, 2), (0, 2), (0, 1), (0, 3), (0, 1), (0, 0), (0, 0), (0, 0), (0, 0)),
+    ((1, 1), (1, 3), (1, 1), (1, 1), (1, 1), (1, 1), (0, 3), (0, 1), (1, 1)),
+    ((2, 2), (2, 2), (2, 2), (2, 2), (2, 2), (2, 3), (0, 3), (2, 2), (2, 2)),
+    ((2, 3), (2, 3), (0, 3), (3, 3), (2, 3), (3, 3), (0, 3), (3, 3), (1, 3)),
+)
+RANKS = (
+    (0.98, 2.75, 3.09, 4.72, 2.28, 7.34, 5.35, 5.05, 5.57),
+    (-0.59, 0.97, 3.70, 3.76, 0.58, 8.74, 11.15, 6.05, 10.14),
+    (2.58, 3.18, 1.14, 4.50, 1.86, 1.38, 1.00, 0.63, 2.20),
+    (4.44, 4.79, 5.54, 4.72, 3.65, 0.90, 4.97, 3.57, 3.69),
+)
+CROSS = (
+    (1.79, 1.76, 1.17, 0.05, -0.15, 1.84, 1.49, 3.23, 0.29),
+    (1.91, 0.67, 1.91, 2.54, 2.95, 0.66, 1.52, 0.56, 2.95),
+    (-0.24, 2.08, 0.64, 2.98, 3.67, -0.32, 1.30, -0.30, 0.21),
+    (0.46, 0.19, 3.29, 3.55, 2.08, 2.08, 1.84, 1.78, -0.37),
+)
+OTHER_SIDE = -0.3
 DOWN = tuple(p for p in range(len(PARTS)) if PARTS[p][0] == "down")
 FAR_GROUPS = ((0, 2), (2, 2))
 NEAR_GROUPS = ((0, 2), (2, 1), (3, 1))
 UNIT, LAG, LEAD = 7.73, 2.0, 16.0
+WAYS = ("up", "dn", "y", "x")
+RING = 6
 
 
 def crossing(src, p, n_z):
     return PARTS[p][0] == "down" and 2 * src >= n_z
 
 
-def reach(src, p, n_z):
-    if crossing(src, p, n_z) or PARTS[p][3] == "a":
-        return (src, src)
-    return (0, n_z - 1)
-
-
 def length(p):
     return UNIT * (0.5 if PARTS[p][0] == "down" else PARTS[p][2] / 8)
 
 
-def rank(n_z, m, link, item):
+def rank(m, link, item):
     src, side, p = item
-    if link == "x":
-        return (0,)
-    b = reach(src, p, n_z) != (src, src)
-    if link == "y" and b:
-        return (0, p)
-    if PARTS[p][0] == "down":
-        return (1 if crossing(src, p, n_z) else 4, p, abs(src - m), side)
-    return (3 if b else 2, p, abs(src - m), side)
+    if link == "y" and REACH[src][p] != (src, src):
+        return CROSS[src][p]
+    return RANKS[src][p] + OTHER_SIDE * side + 0.01 * abs(src - m)
 
 
 def simulate(n_z):
@@ -457,13 +467,13 @@
             add(at + length(item[2]) + LAG, "land", m, link, item)
 
     def put(at, m, link, item):
-        queue[m, link].append((rank(n_z, m, link, item), item))
+        queue[m, link].append((rank(m, link, item), item))
         kick(at, m, link)
 
     def got(at, m, item):
         src, side, p = item
         have[m][item] = at
-        low, high = reach(src, p, n_z)
+        low, high = REACH[src][p]
         if m >= src and m < (n_z - 1 if side == 0 else high):
             put(at, m, "up", item)
         if m <= src and m > (0 if side == 0 else low):
@@ -523,11 +533,11 @@
     before = {}
     for m in range(n_z):
         todo = [(at, 0, "wait", item) for item, at in have[m].items() if item[:2] != (m, 0)]
-        for link in ("up", "dn", "y", "x"):
+        for link in WAYS:
             last = 0.0
-            for at, item in sent[m, link]:
+            for i, (at, item) in enumerate(sent[m, link]):
                 last = max(last, have[m][item], at - LEAD)
-                todo.append((last, 1, link, item))
+                todo.append((last, 1, link, i))
         for item, at in have[m].items():
             if PARTS[item[2]][0] == "down" and not crossing(item[0], item[2], n_z):
                 todo.append((at, 1, "core", item))
@@ -538,13 +548,14 @@
             before[m, step] = [e[2:] for e in todo if e[0] <= now]
             todo = [e for e in todo if e[0] > now]
             now += spans[step[0]]
-    return steps, sources, before
+    items = {key: [item for _, item in log] for key, log in sent.items()}
+    return steps, sources, before, items
 
 
 def line_kernel(
     n_fs, n_tp, tok_hbm, gain, gw_hbm, uw_hbm, dw_hbm, gate_o, up_o, down_o, dcol, hidden, hidden_near, out_in,
     tok, gw, uw, dw, normed, acc_g, acc_u, far_a, far_b, far_in, out_send,
-    in_sem, ag_send, ag_recv, aa_send, aa_recv, fp_send, fp_recv, ac_send, ac_recv, hid_send, hid_recv,
+    in_sem, link_send, core_send, ag_recv, aa_recv, fp_send, fp_recv, ac_send, ac_recv, hid_send, hid_recv,
 ):
     loads = [
         pltpu.make_async_copy(src, dst, in_sem.at[i])
@@ -572,7 +583,7 @@
     near = t + 1 - 2 * (t % 2)
     far = t + 2 - 4 * x
     far_near = far + 1 - 2 * (far % 2)
-    steps, sources, before = timetable(n_z)
+    steps, sources, before, items = timetable(n_z)
 
     def z_of(src):
         return src + x * (n_z - 1 - 2 * src)
@@ -582,39 +593,40 @@
         return 2 * z_of(src) + (y if side == 0 else 1 - y)
 
     def view(o, p):
-        name, first, n, _ = PARTS[p]
+        name, first, n = PARTS[p]
         if name == "down":
             return dcol.at[o, :, pl.ds(first * part, n * part)]
         ref = gate_o if name == "gate" else up_o
         step = rows // 16
         return ref.at[pl.ds(pl.multiple_of(o * rows + first * step, step), n * step), :]
 
-    def ag(item, way, dest):
+    def ag(item, send, dest):
         o, p = owner_of(item), item[2]
         v = view(o, p)
         return pltpu.make_async_remote_copy(
-            v, v, ag_send.at[o, p, way], ag_recv.at[o, p], device_id=(dest, t), device_id_type=MESH,
+            v, v, send, ag_recv.at[o, p], device_id=(dest, t), device_id_type=MESH,
         )
 
-    def hand(item):
+    def hand(item, send):
         o, p = owner_of(item), item[2]
-        _, first, n, _ = PARTS[p]
+        _, first, n = PARTS[p]
+        group = [q <= first < q + m for q, m in FAR_GROUPS].index(True)
+        lane = (t + o // per) % 2 * len(FAR_GROUPS) + group if crossing(item[0], p, n_z) else 2 * len(FAR_GROUPS)
         row = pl.multiple_of((o % per) * d_rows, d_rows)
         col = pl.multiple_of(t * d_cols + first * part, part)
         return pltpu.make_async_remote_copy(
             view(o, p), down_o.at[pl.ds(row, d_rows), pl.ds(col, n * part)],
-            aa_send.at[o, p], aa_recv.at[t, o % per, p],
-            device_id=(f, o // per), device_id_type=MESH,
+            send, aa_recv.at[lane], device_id=(f, o // per), device_id_type=MESH,
         )
 
-    def transfer(what, item):
-        if what == "up":
-            return ag(item, 0, ahead)
-        if what == "dn":
-            return ag(item, 1, behind)
-        if what == "y":
-            return ag(item, 2, other_y)
-        return hand(item)
+    def transfer(m, what, i):
+        item, send = items[m, what][i], link_send.at[WAYS.index(what), i % RING]
+        if what == "x":
+            return hand(item, send)
+        return ag(item, send, {"up": ahead, "dn": behind, "y": other_y}[what])
+
+    def to_core(item):
+        return hand(item, core_send.at[item[1] * len(DOWN) + DOWN.index(item[2])])
 
     def elsewhere(item):
         return owner_of(item) // per != t
@@ -624,11 +636,13 @@
             def events(m=m):
                 for what, item in before[m, step]:
                     if what == "wait":
-                        ag(item, 0, f).wait_recv()
+                        ag(item, link_send.at[0, 0], f).wait_recv()
                     elif what == "core":
-                        pl.when(elsewhere(item))(lambda item=item: hand(item).start())
+                        pl.when(elsewhere(item))(lambda item=item: to_core(item).start())
                     else:
-                        transfer(what, item).start()
+                        if item >= RING:
+                            transfer(m, what, item - RING).wait_send()
+                        transfer(m, what, item).start()
             if before[m, step]:
                 pl.when(place == m)(events)
 
@@ -690,17 +704,11 @@
             v = acc_g[pl.ds(r, 32), :]
             hidden[pl.ds(r, 32), :] = (v / (1.0 + jnp.exp(-v)) * acc_u[pl.ds(r, 32), :]).astype(jnp.bfloat16)
 
-    def arrived(c, q, n):
-        for k in range(per):
-            for p in DOWN:
-                _, first, m, _ = PARTS[p]
-                if q <= first < q + n:
-                    ref = down_o.at[
-                        pl.ds(k * d_rows, d_rows), pl.ds(pl.multiple_of(c * d_cols + first * part, part), m * part)
-                    ]
-                    pltpu.make_async_remote_copy(
-                        ref, ref, aa_send.at[0, p], aa_recv.at[c, k, p], device_id=(f, near), device_id_type=MESH,
-                    ).wait_recv()
+    def arrived(c, q, n, lane):
+        ref = down_o.at[:, pl.ds(pl.multiple_of(c * d_cols + q * part, part), n * part)]
+        pltpu.make_async_remote_copy(
+            ref, ref, link_send.at[0, 0], aa_recv.at[lane], device_id=(f, near), device_id_type=MESH,
+        ).wait_recv()
 
     def product(c, q, n, out):
         @pl.loop(0, n_tok // m_tile)
@@ -736,10 +744,10 @@
 
     def far_step(i):
         q, n = FAR_GROUPS[i]
-        arrived(far_near, q, n)
+        arrived(far_near, q, n, len(FAR_GROUPS) + i)
         product(far_near, q, n, far_a.at[:, cols(q, n)])
         far_pair(i).start()
-        arrived(far, q, n)
+        arrived(far, q, n, i)
         product(far, q, n, far_b.at[:, cols(q, n)])
         far_pair(i).wait_recv()
         out_send[:, cols(q, n)] = (
@@ -754,7 +762,7 @@
             down_o[k * d_rows : (k + 1) * d_rows, pl.ds(col, n * part)] = dcol[t * per + k, :, cols(q, n)]
 
     def end():
-        arrived(near, 0, 4)
+        arrived(near, 0, 4, 2 * len(FAR_GROUPS))
         for i in range(len(FAR_GROUPS)):
             across(i).wait_recv()
         hidden_copy().wait_recv()
@@ -790,12 +798,14 @@
     for m in range(n_z):
         @pl.when(place == m)
         def _(m=m):
+            for what in WAYS:
+                count = len(items[m, what])
+                for i in range(max(0, count - RING), count):
+                    transfer(m, what, i).wait_send()
             for step in steps:
                 for what, item in before[m, step]:
                     if what == "core":
-                        pl.when(elsewhere(item))(lambda item=item: hand(item).wait_send())
-                    elif what != "wait":
-                        transfer(what, item).wait_send()
+                        pl.when(elsewhere(item))(lambda item=item: to_core(item).wait_send())
 
 
 def finish(
@@ -861,10 +871,10 @@
             pltpu.VMEM((n_tok, width), jnp.float32),
             *[pltpu.VMEM((n_tok, d_cols), bf)] * 4,
             dma((4,)),
-            dma((n_fs, n_p, 3)),
+            dma((len(WAYS), RING)),
+            dma((2 * len(DOWN),)),
             dma((n_fs, n_p)),
-            dma((n_fs, n_p)),
-            dma((n_tp, n_fs // n_tp, n_p)),
+            dma((2 * n_far + 1,)),
             dma((n_far,)),
             dma((n_far,)),
             dma((n_far,)),

time: 187 us -> 179 us (0.957)
  Pallas kernels: 185 us -> 177 us
    pallas_call x1, Pallas kernels: 178 us -> 171 us  [line_on_device(): pl.pallas_call(functools.partial(line_kernel, n_fs, n_tp), out_shape=tupl...]
where the time goes in v3:
time: 179 us; the launch traced here: 178 us
  Pallas kernels  177 us (99%)
    pallas_call x1, Pallas kernels, line_on_device(): pl.pallas_call(functools.partial(line_kernel, n_fs, n_tp), out_shape=tupl...  171 us
    pallas_call x1, Pallas kernels, line_on_device(): pl.pallas_call(functools.partial(finish, n_tp), out_shape=tuple((jax.Shap...  6.28 us

profile of v3, /device:TPU:0, one launch (start us, length us, event | category | flops | bytes accessed | tf_op | source)
XLA Modules:
  0.0 177.8 jit_solution(17306501221307283013)
XLA Ops:
  0.6 170.9 %shard_map.84 = (bf16[2048,1408]{1,0:T(8,128)(2,1)S(1)}, bf16[2048,1408]{1,0:T(8,128)(2,1)S(1)}, bf16[1408,2048]{1,0:T(8,128)(2,1)S(1)}, bf16[8,704,512]{2,1,0:T...) custom-call(bf16[768,2048]{1,0:T(8,128)(2,1)} %tok_hbm.1, ...), custom_call_target="tpu_custom_call" | custom-call | tf_op jit(solution)/shard_map/pallas_call | solution.py:859
  171.6 6.3 %shard_map.85 = (bf16[2048,1408]{1,0:T(8,128)(2,1)}, bf16[2048,1408]{1,0:T(8,128)(2,1)}, bf16[1408,2048]{1,0:T(8,128)(2,1)}, bf16[768,512]{1,0:T(8,128)(2,1)}) custom-call(bf16[2048,1408]{1,0:T(8,128)(2,1)S(1)} %get-tuple-element.11.gate_i, bf16[2048,1408]{1,0:T(8,128)(2,1)S(1)} %get-tuple-element.12.up_i, bf16[1408,2048]{1,0:T(8,128)(2,1)S(1)} %get-tuple-element.13.down_i, ...), custom_call_target="tpu_custom_call" | custom-call | tf_op jit(solution)/shard_map/pallas_call | solution.py:889

commit v4 on v3

--- a/solution.py
+++ b/solution.py
@@ -424,7 +424,7 @@
 DOWN = tuple(p for p in range(len(PARTS)) if PARTS[p][0] == "down")
 FAR_GROUPS = ((0, 2), (2, 2))
 NEAR_GROUPS = ((0, 2), (2, 1), (3, 1))
-UNIT, LAG, LEAD = 7.73, 2.0, 16.0
+UNIT, LAG, LEAD = 7.73, 2.0, 10.0
 WAYS = ("up", "dn", "y", "x")
 RING = 6
 
@@ -595,7 +595,7 @@
     def view(o, p):
         name, first, n = PARTS[p]
         if name == "down":
-            return dcol.at[o, :, pl.ds(first * part, n * part)]
+            return dcol.at[o, first]
         ref = gate_o if name == "gate" else up_o
         step = rows // 16
         return ref.at[pl.ds(pl.multiple_of(o * rows + first * step, step), n * step), :]
@@ -661,7 +661,8 @@
     loads[0].wait()
     gate_o[pl.ds(base, rows), :] = (gw[...] * g).astype(jnp.bfloat16)
     loads[1].wait()
-    dcol[f] = dw[...].astype(jnp.bfloat16)
+    for j in range(4):
+        dcol[f, j] = dw[:, j * part : (j + 1) * part].astype(jnp.bfloat16)
     inner = jnp.logical_and(z > 0, z < n_z - 1)
     pl.when(inner)(lambda: pl.semaphore_wait(barrier, len(peers)))
     pl.when(jnp.logical_not(inner))(lambda: pl.semaphore_wait(barrier, len(peers) - 1))
@@ -757,9 +758,10 @@
 
     def near_step(i):
         q, n = NEAR_GROUPS[i]
-        col = pl.multiple_of(t * d_cols + q * part, part)
-        for k in range(per):
-            down_o[k * d_rows : (k + 1) * d_rows, pl.ds(col, n * part)] = dcol[t * per + k, :, cols(q, n)]
+        for j in range(q, q + n):
+            col = pl.multiple_of(t * d_cols + j * part, part)
+            for k in range(per):
+                down_o[k * d_rows : (k + 1) * d_rows, pl.ds(col, part)] = dcol[t * per + k, j]
 
     def end():
         arrived(near, 0, 4, 2 * len(FAR_GROUPS))
@@ -814,7 +816,8 @@
     t = lax.axis_index("tp")
     near = t + 1 - 2 * (t % 2)
     per = dcol.shape[0] // n_tp
-    d_rows, d_cols = dcol.shape[1:]
+    parts, d_rows, part = dcol.shape[1:]
+    d_cols = parts * part
     n_tok = hidden.shape[0]
     m_tile = min(256, n_tok)
     copies = [
@@ -824,7 +827,8 @@
     for copy in copies[:3]:
         copy.start()
     for k in range(per):
-        near_w[k * d_rows : (k + 1) * d_rows, :] = dcol[near * per + k]
+        for j in range(parts):
+            near_w[k * d_rows : (k + 1) * d_rows, j * part : (j + 1) * part] = dcol[near * per + k, j]
     col = pl.multiple_of(t * d_cols, d_cols)
 
     @pl.loop(0, n_tok // m_tile)
@@ -853,7 +857,7 @@
     hbm = pl.BlockSpec(memory_space=pl.ANY)
     d_own = d_rows * n_fs // n_tp
     shapes = (
-        (d_model, width), (d_model, width), (d_own, d_model), (n_fs, d_rows, d_cols),
+        (d_model, width), (d_model, width), (d_own, d_model), (n_fs, 4, d_rows, d_cols // 4),
         (n_tok, width), (n_tok, width), (n_tok, d_cols),
     )
     held = pl.pallas_call(

time: 179 us -> 179 us (level)
  no operation moved by 1% of the time
where the time goes in v4:
time: 179 us; the launch traced here: 178 us
  Pallas kernels  177 us (99%)
    pallas_call x1, Pallas kernels, line_on_device(): pl.pallas_call(functools.partial(line_kernel, n_fs, n_tp), out_shape=tupl...  171 us
    pallas_call x1, Pallas kernels, line_on_device(): pl.pallas_call(functools.partial(finish, n_tp), out_shape=tuple((jax.Shap...  6.28 us

profile of v4, /device:TPU:0, one launch (start us, length us, event | category | flops | bytes accessed | tf_op | source)
XLA Modules:
  0.0 177.9 jit_solution(14016046072534307348)
XLA Ops:
  0.6 171.0 %shard_map.84 = (bf16[2048,1408]{1,0:T(8,128)(2,1)S(1)}, bf16[2048,1408]{1,0:T(8,128)(2,1)S(1)}, bf16[1408,2048]{1,0:T(8,128)(2,1)S(1)}, bf16[8,4,704,128]{3,2,1...) custom-call(bf16[768,2048]{1,0:T(8,128)(2,1)} %tok_hbm.1, ...), custom_call_target="tpu_custom_call" | custom-call | tf_op jit(solution)/shard_map/pallas_call | solution.py:863
  171.6 6.3 %shard_map.85 = (bf16[2048,1408]{1,0:T(8,128)(2,1)}, bf16[2048,1408]{1,0:T(8,128)(2,1)}, bf16[1408,2048]{1,0:T(8,128)(2,1)}, bf16[768,512]{1,0:T(8,128)(2,1)}) custom-call(bf16[2048,1408]{1,0:T(8,128)(2,1)S(1)} %get-tuple-element.11.gate_i, bf16[2048,1408]{1,0:T(8,128)(2,1)S(1)} %get-tuple-element.12.up_i, bf16[1408,2048]{1,0:T(8,128)(2,1)S(1)} %get-tuple-element.13.down_i, ...), custom_call_target="tpu_custom_call" | custom-call | tf_op jit(solution)/shard_map/pallas_call | solution.py:893
